TPU v7x, 128 devices: a 2x2x16 block of a 8x8x16 slice. The times are simulated.
128 devices in a mesh: grp: 4 (over y, x), ep: 32 (over z, core).
Axes of the slice: x: 2, y: 2, z: 16, core: 2. Of those that a mesh axis runs over, the one named last changes fastest.
The devices are a block of a 8x8x16 slice.
Arguments:
- tokens: bfloat16 [4096, 2048], P(('grp', 'ep')), parts along dimension 0, may hold values from -6 to 6
- routes: int32 [4096, 4], P(('grp', 'ep')), parts along dimension 0, may hold values from 0 to 31, all different within a row; in each aligned block of 32 rows (0 to 31, 32 to 63, ...) at most 8 rows name the same one
- in_gain: float32 [2048], replicated, may hold values from 0.1 to 1.9
- group_router: float32 [2048, 4], replicated, may hold values from -0.03125 to 0.03125
- expert_router: float32 [2048, 32], replicated, may hold values from -0.03125 to 0.03125
- w_gate: bfloat16 [32, 2048, 512], P('ep'), may hold values from -0.125 to 0.125
- w_up: bfloat16 [32, 2048, 512], P('ep'), may hold values from -0.125 to 0.125
- w_down: bfloat16 [32, 512, 2048], P('ep')
- out_gain: float32 [2048], P('ep'), may hold values from 0.1 to 1.9
Outputs:
- mixed_out: bfloat16 [4096, 2048], P('grp', 'ep'), parts along dimension 0
There are 4 independent parts, one for each index of `grp`. A program takes and returns all parts, laid end to end along the dimension named above; an argument that names none is the same for every part. Nothing has to cross between parts.
Inputs may be any that keep to these rules, and one draw needn't show every extreme that they name: `routes`: each row names 4 different experts; in the rows of one device no expert is named more than 8 times, a bound that some block reaches.
All inputs are finite; a program needn't handle non-finite values.
Results may differ from a plain program's by a relative error of at most 0.0085.
Values may be sent and summed in bfloat16 or wider, within the bound.
A program may use at most 64 MiB of HBM per device.

v0:
```python
import jax
import jax.numpy as jnp
from jax import lax
from jax.sharding import PartitionSpec as P

EPSILON = 1e-06


def normalize(tokens, in_gain):
    values = tokens.astype(jnp.float32)
    scaled = values * lax.rsqrt(jnp.mean(values * values, axis=1, keepdims=True) + EPSILON)
    return (scaled * in_gain).astype(jnp.bfloat16)


def gate_values(normed, routes, group_router, expert_router):
    wide = normed.astype(jnp.float32)
    group_logit = jnp.dot(wide, group_router, precision=lax.Precision.HIGHEST)
    expert_logit = jnp.dot(wide, expert_router, precision=lax.Precision.HIGHEST)
    group_prob = jnp.exp(group_logit) / jnp.sum(jnp.exp(group_logit), axis=1, keepdims=True)
    chosen = jnp.exp(jnp.take_along_axis(expert_logit, routes, axis=1))
    expert_prob = chosen / jnp.sum(chosen, axis=1, keepdims=True)
    per_group = expert_router.shape[1] // group_router.shape[1]
    return jnp.take_along_axis(group_prob, routes // per_group, axis=1) * expert_prob


def slot_order(pairs, experts):
    onehot = (pairs[:, :, None] == jnp.arange(experts, dtype=jnp.int32)).astype(jnp.int32)
    return jnp.sum(onehot * (jnp.cumsum(onehot, axis=1) - 1), axis=2)


def expert_rows(rows, w_gate, w_up, w_down):
    gate = jnp.dot(rows, w_gate[0], preferred_element_type=jnp.float32)
    upward = jnp.dot(rows, w_up[0], preferred_element_type=jnp.float32)
    hidden = (jax.nn.silu(gate) * upward).astype(jnp.bfloat16)
    return jnp.dot(hidden, w_down[0], preferred_element_type=jnp.float32).astype(jnp.bfloat16)


def per_device(
    tokens, routes, in_gain, group_router, expert_router, w_gate, w_up, w_down, out_gain
):
    tok_dev, top_count = routes.shape
    experts = expert_router.shape[1]
    capacity = 2 * tok_dev * top_count // experts
    normed = normalize(tokens, in_gain)
    weights = gate_values(normed, routes, group_router, expert_router)
    flat_route = routes.reshape(-1)
    order_in = slot_order(flat_route[None, :], experts)[0]
    slot_index = flat_route * capacity + order_in
    token_index = jnp.arange(tok_dev * top_count, dtype=jnp.int32) // top_count
    table = jnp.zeros((experts * capacity,), jnp.int32).at[slot_index].set(token_index)
    filled = jnp.zeros((experts * capacity,), jnp.bool_).at[slot_index].set(True)
    outgoing = jnp.where(filled[:, None], normed[table], jnp.zeros((), jnp.bfloat16))
    outgoing = outgoing.reshape(experts, capacity, normed.shape[1])
    arrived = lax.all_to_all(outgoing, "ep", split_axis=0, concat_axis=0, tiled=True)
    flat_rows = arrived.reshape(-1, arrived.shape[2])
    answer = expert_rows(flat_rows, w_gate, w_up, w_down).reshape(arrived.shape)
    returned = lax.all_to_all(answer, "ep", split_axis=0, concat_axis=0, tiled=True)
    pair_rows = returned.reshape(experts * capacity, normed.shape[1])[slot_index]
    weighted = pair_rows.astype(jnp.float32) * weights.reshape(-1)[:, None]
    mixed = jnp.sum(weighted.reshape(tok_dev, top_count, normed.shape[1]), axis=1)
    local_scale = lax.rsqrt(jnp.mean(mixed * mixed, axis=1, keepdims=True) + EPSILON)
    sending = mixed * local_scale
    part = lax.all_to_all(
        sending.astype(jnp.bfloat16), "ep", split_axis=1, concat_axis=0, tiled=True
    ).astype(sending.dtype)
    return (part * out_gain).astype(jnp.bfloat16)


def solution(mesh):
    in_specs = (
        P(("grp", "ep"), None),
        P(("grp", "ep"), None),
        P(),
        P(),
        P(),
        P("ep", None, None),
        P("ep", None, None),
        P("ep", None, None),
        P("ep"),
    )
    out_specs = P("grp", "ep")
    return jax.shard_map(
        per_device, mesh=mesh, in_specs=in_specs, out_specs=out_specs, check_vma=False
    )
```

profile of v0, /device:TPU:69, one launch (start us, length us, event | category | flops | bytes accessed | tf_op | source)
XLA Modules:
  0.0 173.3 jit_solution(1757881125333152523)
XLA Ops:
  0.0 0.8 broadcast_multiply_fusion
  0.8 0.8 copy.54
  1.6 1.0 fusion.24
  3.4 1.0 scatter_custom_fusion.1
  4.4 1.0 scatter_custom_fusion
  5.5 1.0 fusion.26
  6.6 1.4 gather_fusion
  8.1 73.9 %all_to_all.20 = bf16[32,8,2048]{2,1,0:T(8,128)(2,1)S(1)} all-to-all(bf16[32,8,2048]{2,1,0:T(8,128)(2,1)S(1)} %bitcast_select_fusion), channel_id=1, replica_groups=mesh['grp'=4,'ep'=32] {'ep'}, dimensions={0} | all-to-all | bytes 2097152 | tf_op jit(solution)/shard_map/all_to_all | solution.py:54
  82.0 1.6 fusion.4
  83.6 4.0 %fusion = bf16[32,8,2048]{2,1,0:T(8,128)(2,1)} fusion(bf16[1,512,2048]{2,1,0:T(8,128)(2,1)S(1)} %copy-done, bf16[1,2048,512]{2,1,0:T(8,128)(2,1)} %param.15, bf16[32,8,2048]{2,1,0:T(8,128)(2,1)S(1)} %all_to_all.20, f32[256,512]{1,0:T(8,128)} %fusion.4), kind=kOutput, calls=%fused_computation.7 | convolution fusion | flops 1075052544 | bytes 6815744 | tf_op jit(solution)/shard_map/dot_general | solution.py:35
  87.6 4.5 %all-to-all-start.1 = ((bf16[32,8,2048]{2,1,0:T(8,128)(2,1)}), bf16[32,8,2048]{2,1,0:T(8,128)(2,1)S(1)}, u32[]{:S(2)}, u32[]{:S(2)}) async-start(bf16[32,8,2048]{2,1,0:T(8,128)(2,1)} %fusion), calls=%async_computation.1 | async-start | bytes 2097152 | tf_op jit(solution)/shard_map/all_to_all | solution.py:57
  92.5 0.2 fusion.38
  92.8 1.5 gather_fusion.2
  94.5 1.2 fusion.39
  95.6 1.3 gather_fusion.3
  97.3 50.4 %all-to-all-done.1 = bf16[32,8,2048]{2,1,0:T(8,128)(2,1)S(1)} async-done(((bf16[32,8,2048]{2,1,0:T(8,128)(2,1)}), bf16[32,8,2048]{2,1,0:T(8,128)(2,1)S(1)}, u32[]{:S(2)}, u32[]{:S(2)}) %all-to-all-start.1) | async-done | bytes 1048608 | tf_op jit(solution)/shard_map/all_to_all | solution.py:57
  147.7 1.7 gather_fusion.1
  149.4 1.4 reshape.225
  150.8 0.7 multiply_reduce_fusion
  151.7 0.2 reduce_sum.64
  152.1 0.2 reshape.286
  152.3 19.9 %all_to_all.21 = bf16[32,2,1024]{2,1,0:T(2,128)(2,1)S(1)} all-to-all(bf16[32,2,1024]{2,1,0:T(2,128)(2,1)S(1)} %reshape.286), channel_id=1, replica_groups=mesh['grp'=4,'ep'=32] {'ep'}, dimensions={0} | all-to-all | bytes 262144 | tf_op jit(solution)/shard_map/all_to_all | solution.py:63
  172.2 0.2 reshape.287
  172.5 0.8 copy.61
  (43 shorter events, 2.3 us)
Async XLA Ops:
  0.0 83.6 %copy-start = (bf16[1,512,2048]{2,1,0:T(8,128)(2,1)S(1)}, bf16[1,512,2048]{2,1,0:T(8,128)(2,1)}, u32[]{:S(2)}) copy-start(bf16[1,512,2048]{2,1,0:T(8,128)(2,1)} %param.16) | copy-start | bytes 6291460
  7.9 74.1 %copy-start.4 = (bf16[1,2048,512]{2,1,0:T(8,128)(2,1)S(1)}, bf16[1,2048,512]{2,1,0:T(8,128)(2,1)}, u32[]{:S(2)}) copy-start(bf16[1,2048,512]{2,1,0:T(8,128)(2,1)} %param.14) | copy-start | bytes 6291460
  87.6 4.5 %copy-start.1 = (s32[32,4]{0,1:T(4,128)S(1)}, s32[32,4]{0,1:T(4,128)}, u32[]{:S(2)}) copy-start(s32[32,4]{0,1:T(4,128)} %param.10) | copy-start | bytes 1540
  87.6 4.9 %copy-start.2 = (f32[2048,4]{0,1:T(4,128)S(1)}, f32[2048,4]{0,1:T(4,128)}, u32[]{:S(2)}) copy-start(f32[2048,4]{0,1:T(4,128)} %param.12) | copy-start | bytes 98308
  87.6 60.1 %all-to-all-start.1 = ((bf16[32,8,2048]{2,1,0:T(8,128)(2,1)}), bf16[32,8,2048]{2,1,0:T(8,128)(2,1)S(1)}, u32[]{:S(2)}, u32[]{:S(2)}) async-start(bf16[32,8,2048]{2,1,0:T(8,128)(2,1)} %fusion), calls=%async_computation.1 | async-start | bytes 2097152 | tf_op jit(solution)/shard_map/all_to_all | solution.py:57
  150.8 21.7 %copy-start.3 = (f32[64]{0:T(128)S(1)}, f32[64]{0:T(128)}, u32[]{:S(2)}) copy-start(f32[64]{0:T(128)} %param.17) | copy-start | bytes 772
where the time goes:
time: 174 us; the launch traced here: 173 us
  blocking collectives  93.8 us (54%)
  waiting for transfers between devices  50.4 us (29%)
  local copies, waits for them, and re-layouts  12.8 us (7%)
  matrix products  6.98 us (4%)
  other arithmetic  4.58 us (3%)
  starting transfers between devices  4.46 us (3%)
    all_to_all x1, blocking collectives, per_device(): lax.all_to_all(outgoing, 'ep', split_axis=0, concat_axis=0, tiled=True)  73.9 us
    all_to_all x1, waiting for transfers between devices, per_device(): lax.all_to_all(answer, 'ep', split_axis=0, concat_axis=0, tiled=True)  50.4 us
    all_to_all x1, blocking collectives, per_device(): lax.all_to_all(sending.astype(jnp.bfloat16), 'ep', split_axis=1, concat_a...  19.9 us
    all_to_all x1, starting transfers between devices, per_device(): lax.all_to_all(answer, 'ep', split_axis=0, concat_axis=0, tiled=True)  4.46 us
    dot_general x1, matrix products, expert_rows(): jnp.dot(hidden, w_down[0], preferred_element_type=jnp.float32)  4.01 us
  transfers between devices with their start and end apart: 1, of which 1 were waited for; matrix products, arithmetic and copies ran while one was open for 3% of the time, Pallas kernels for 0%

commit v1 on v0

v1 whole, which is shorter than its diff:
```python
import functools

import jax
import jax.numpy as jnp
from jax import lax
from jax.experimental import pallas as pl
from jax.experimental.pallas import tpu as pltpu
from jax.sharding import PartitionSpec as P

EPSILON = 1e-06
MESH = pl.DeviceIdType.MESH
F32 = jnp.float32
BF16 = jnp.bfloat16
LANES = 128


def layer_kernel(
    n_ep,
    tok_hbm, routes_hbm, gain_hbm, gr_hbm, er_hbm, wg_hbm, wu_hbm, wd_hbm, og_hbm,
    out_ref,
    tok, rts, gain, rtr, og, wg, wu, wd,
    own, oth, own_w, oth_w,
    gate_s, hid_s, y_own, y_snd, y_rcv,
    rs_s, rs_r, mix, mix_t, stat, total,
    in_sem, w_sem,
    ag_recv, agw_recv, dd_recv, ddw_recv, y_recv, rs_recv, mix_recv, stat_recv, tot_recv,
    ag_send, agw_send, dd_send, ddw_send, y_send, rs_send, mix_send, stat_send, tot_send,
):
    chips = n_ep // 2
    half = chips // 2
    rows, width = tok.shape
    experts = n_ep
    me = lax.axis_index("ep")
    z, c = me // 2, me % 2
    right, left = (me + 2) % n_ep, (me + n_ep - 2) % n_ep
    partner = me + 1 - 2 * c
    sides = (right, left)

    def remote(src, dst, send, recv, to):
        return pltpu.make_async_remote_copy(
            src_ref=src, dst_ref=dst, send_sem=send, recv_sem=recv,
            device_id={"ep": to}, device_id_type=MESH,
        )

    def wait(ref, sem):
        pltpu.make_async_copy(ref, ref, sem).wait()

    barrier = pltpu.get_barrier_semaphore()
    for peer in (right, left, partner):
        pl.semaphore_signal(barrier, inc=1, device_id={"ep": peer}, device_id_type=MESH)

    first = [(tok_hbm, tok), (gain_hbm, gain)]
    second = [
        (er_hbm, rtr.at[pl.ds(0, experts)]),
        (gr_hbm, rtr.at[pl.ds(experts, gr_hbm.shape[0])]),
        (routes_hbm, rts),
        (og_hbm, og),
    ]
    loads = [pltpu.make_async_copy(s, d, in_sem.at[i]) for i, (s, d) in enumerate(first + second)]
    for copy in loads:
        copy.start()
    big = [
        pltpu.make_async_copy(s, d, w_sem.at[i])
        for i, (s, d) in enumerate([(wg_hbm, wg), (wu_hbm, wu), (wd_hbm, wd)])
    ]
    for copy in big:
        copy.start()

    loads[0].wait()
    loads[1].wait()
    values = tok[...].astype(F32)
    scaled = values * lax.rsqrt(jnp.mean(values * values, axis=1, keepdims=True) + EPSILON)
    own[z] = (scaled * gain[...]).astype(BF16)
    pl.semaphore_wait(barrier, 3)

    subs = 4

    def piece(ref, slot, sub):
        a, b = sub // 2, sub % 2
        return ref.at[slot, pl.ds(a * (rows // 2), rows // 2), pl.ds(b * (width // 2), width // 2)]

    def slot_of(side, step):
        return (z + chips - step) % chips if side == 0 else (z + step) % chips

    def has_piece(side, step, sub):
        return step < half or (sub < subs // 2) == (side == 0)

    def forward(side, step, sub):
        slot = slot_of(side, step)
        remote(
            piece(own, slot, sub), piece(own, slot, sub),
            ag_send, ag_recv.at[side, step, sub], sides[side],
        ).start()

    def forward_w(side, step):
        slot = slot_of(side, step)
        remote(own_w.at[slot], own_w.at[slot], agw_send, agw_recv.at[side, step], sides[side]).start()

    def across(slot):
        remote(own.at[slot], oth.at[slot], dd_send, dd_recv.at[slot], partner).start()

    def across_w(slot):
        remote(own_w.at[slot], oth_w.at[slot], ddw_send, ddw_recv.at[slot], partner).start()

    for sub in range(subs):
        for side in range(2):
            forward(side, 0, sub)
    across(z)

    for copy in loads[2:]:
        copy.wait()
    mine = own[z]
    table = rtr[...]
    row_id = lax.broadcasted_iota(jnp.int32, table.shape, 0)
    table = jnp.where(row_id < experts + gr_hbm.shape[0], table, 0.0)
    high = table.astype(BF16)
    rest = table - high.astype(F32)
    middle = rest.astype(BF16)
    low = (rest - middle.astype(F32)).astype(BF16)
    repeats = LANES // rows
    wide = jnp.concatenate([mine] * repeats, axis=0)
    dims = (((1,), (1,)), ((), ()))
    logit = sum(
        lax.dot_general(part, wide, dims, preferred_element_type=F32) for part in (low, middle, high)
    )
    groups = gr_hbm.shape[0]
    per_group = experts // groups
    expert_exp = jnp.exp(logit[:experts])
    group_exp = jnp.exp(logit[experts:experts + groups])
    group_prob = group_exp / jnp.sum(group_exp, axis=0, keepdims=True)
    group_wide = jnp.concatenate(
        [jnp.broadcast_to(group_prob[g:g + 1], (per_group, LANES)) for g in range(groups)], axis=0
    )
    top = rts.shape[0]
    spread = (
        lax.broadcasted_iota(jnp.int32, (rows, LANES), 1) % rows
        == lax.broadcasted_iota(jnp.int32, (rows, LANES), 0)
    )
    chosen = jnp.dot(
        rts[...].astype(F32).astype(BF16), spread.astype(F32).astype(BF16), preferred_element_type=F32
    )
    expert_id = lax.broadcasted_iota(jnp.int32, (experts, LANES), 0).astype(F32)
    named = expert_id == chosen[0:1]
    for j in range(1, top):
        named = named | (expert_id == chosen[j:j + 1])
    picked = jnp.where(named, expert_exp, 0.0)
    weight = group_wide * (picked / jnp.sum(picked, axis=0, keepdims=True))
    lane_block = lax.broadcasted_iota(jnp.int32, (8, LANES), 1) // rows
    packed = weight[0:8]
    for g in range(1, experts // 8):
        packed = jnp.where(lane_block == g, weight[8 * g:8 * g + 8], packed)
    own_w[z] = packed
    for copy in big:
        copy.wait()
    for side in range(2):
        forward_w(side, 0)
    across_w(z)

    def weight_column(ref, slot):
        line = ref[slot, pl.ds(me % 8, 1), :]
        lane = lax.broadcasted_iota(jnp.int32, (rows, LANES), 1)
        token = lax.broadcasted_iota(jnp.int32, (rows, LANES), 0)
        hit = lane == token + rows * (me // 8)
        return jnp.sum(jnp.where(hit, jnp.broadcast_to(line, (rows, LANES)), 0.0), axis=1, keepdims=True)

    def slots_of(step):
        if step == 0 or step == half:
            return [slot_of(0, step)]
        return [slot_of(0, step), slot_of(1, step)]

    def block(step):
        slots = slots_of(step)
        count = 2 * len(slots) * rows

        def tokens_in():
            return jnp.concatenate([own[k] for k in slots] + [oth[k] for k in slots], axis=0)

        def part_gate():
            for k in slots:
                wait(oth.at[k], dd_recv.at[k])
            gate_s[pl.ds(0, count)] = jnp.dot(tokens_in(), wg[0], preferred_element_type=F32)

        def part_up():
            for k in slots:
                wait(oth_w.at[k], ddw_recv.at[k])
            upward = jnp.dot(tokens_in(), wu[0], preferred_element_type=F32)
            gate = gate_s[pl.ds(0, count)]
            column = jnp.concatenate(
                [weight_column(own_w, k) for k in slots] + [weight_column(oth_w, k) for k in slots], axis=0
            )
            hidden = gate / (1.0 + jnp.exp(-gate)) * upward
            hid_s[pl.ds(0, count)] = (hidden * column).astype(BF16)

        def part_down(b):
            cols = pl.ds(b * (width // 2), width // 2)
            y = jnp.dot(hid_s[pl.ds(0, count)], wd[0, :, cols], preferred_element_type=F32)
            for i, k in enumerate(slots):
                y_own[k, :, cols] = y[i * rows:(i + 1) * rows]
                j = i + len(slots)
                y_snd[k, :, cols] = y[j * rows:(j + 1) * rows].astype(BF16)
            if b == 1:
                for k in slots:
                    remote(y_snd.at[k], y_rcv.at[k], y_send, y_recv, partner).start()

        return [part_gate, part_up, lambda: part_down(0), lambda: part_down(1)]

    for step in range(1, half + 1):
        work = block(step - 1)
        for sub in range(subs):
            for side in range(2):
                if has_piece(side, step, sub):
                    slot = slot_of(side, step)
                    wait(piece(own, slot, sub), ag_recv.at[side, step - 1, sub])
                    if step < half and has_piece(side, step + 1, sub):
                        forward(side, step, sub)
            if sub == subs - 1:
                for side in range(2):
                    if step < half or side == 0:
                        slot = slot_of(side, step)
                        wait(own_w.at[slot], agw_recv.at[side, step - 1])
                        if step < half - 1 or (step == half - 1 and side == 0):
                            forward_w(side, step)
                        across(slot)
                        across_w(slot)
            work[sub]()
    for part in block(half):
        part()
    wait(y_rcv, y_recv)

    group_slots = chips // subs

    def mine_of(dest, sub):
        at = pl.ds(sub * group_slots, group_slots)
        cols = pl.ds(pl.multiple_of(dest * LANES, LANES), LANES)
        return y_own[at, :, cols] + y_rcv[at, :, cols].astype(F32)

    def buffer_of(side, step, sub):
        return (side * half + step) * subs + sub

    def starts(side, sub):
        return (sub < subs // 2) == (side == 0)

    for step in range(half):
        for turn in range(subs):
            for side in range(2):
                sub = (turn + (subs // 2) * (side + (step > 0))) % subs
                if step == 0 and not starts(side, sub):
                    continue
                dest = (z + half - step) % chips if side == 0 else (z + half + step) % chips
                value = mine_of(dest, sub)
                if step > 1 or (step == 1 and starts(side, sub)):
                    before = buffer_of(side, step - 1, sub)
                    wait(rs_r.at[before], rs_recv.at[before])
                    value = value + rs_r[before].astype(F32)
                at = buffer_of(side, step, sub)
                rs_s[at] = value.astype(BF16)
                remote(rs_s.at[at], rs_r.at[at], rs_send, rs_recv.at[at], sides[side]).start()

    lines = []
    for turn in range(subs):
        sub = (turn + subs // 2) % subs
        value = mine_of(z, sub)
        for side in range(2):
            last = buffer_of(side, half - 1, sub)
            wait(rs_r.at[last], rs_recv.at[last])
            value = value + rs_r[last].astype(F32)
        mix[c, pl.ds(sub * group_slots, group_slots)] = value
        flat = value.reshape(group_slots * rows, LANES)
        stat[z, pl.ds(sub, 1), :] = jnp.sum(jnp.transpose(flat * flat), axis=0, keepdims=True)

    remote(mix.at[c], mix.at[c], mix_send, mix_recv, partner).start()
    for hop in range(1, chips):
        to = (me + 2 * hop) % n_ep
        remote(stat.at[z], stat.at[z], stat_send, stat_recv, to).start()

    wait(mix.at[1 - c], mix_recv)
    feats = out_ref.shape[0]
    for sub in range(subs):
        flat = jnp.concatenate(
            [mix[h, sub * group_slots + j] for j in range(group_slots) for h in range(2)], axis=0
        )
        turned = jnp.transpose(flat)
        mix_t[:, pl.ds(sub * 2 * LANES, 2 * LANES)] = jnp.where(c == 0, turned[:feats], turned[feats:])
    eye = (
        lax.broadcasted_iota(jnp.int32, (feats, feats), 0)
        == lax.broadcasted_iota(jnp.int32, (feats, feats), 1)
    )
    out_gain = jnp.sum(
        jnp.where(eye, jnp.broadcast_to(og[...], (feats, feats)), 0.0), axis=1, keepdims=True
    )

    wait(stat.at[pl.ds(0, chips - 1)], stat_recv)
    total[c] = jnp.sum(stat[...], axis=0)
    remote(total.at[c], total.at[c], tot_send, tot_recv, partner).start()
    wait(total.at[1 - c], tot_recv)
    scale = lax.rsqrt(total[...] / width + EPSILON)
    s0, s1 = scale[0], scale[1]
    spot = lax.broadcasted_iota(jnp.int32, s0.shape, 1) // rows

    def woven(base):
        turns = [(LANES - base) % LANES, (rows - base) % LANES, (2 * rows - base) % LANES]
        a = pltpu.roll(s0, turns[0], 1) if turns[0] else s0
        b = pltpu.roll(s1, turns[1], 1) if turns[1] else s1
        d = pltpu.roll(s0, turns[1], 1) if turns[1] else s0
        e = pltpu.roll(s1, turns[2], 1) if turns[2] else s1
        return jnp.where(spot == 0, a, jnp.where(spot == 1, b, jnp.where(spot == 2, d, e)))

    first_half, second_half = woven(0), woven(LANES // 2)
    for sub in range(subs):
        for part, lines in enumerate((first_half, second_half)):
            cols = pl.ds((2 * sub + part) * LANES, LANES)
            out_ref[:, cols] = (mix_t[:, cols] * lines[sub:sub + 1] * out_gain).astype(BF16)

    wait(own.at[pl.ds(0, chips - 1)], ag_send)
    wait(own_w.at[pl.ds(0, chips - 1)], agw_send)
    wait(own, dd_send)
    wait(own_w, ddw_send)
    wait(y_snd, y_send)
    wait(rs_s.at[pl.ds(0, (chips - 1) * subs)], rs_send)
    wait(mix.at[c], mix_send)
    wait(stat.at[pl.ds(0, chips - 1)], stat_send)
    wait(total.at[c], tot_send)


def solution(mesh):
    n_ep = mesh.shape["ep"]
    chips = n_ep // 2

    def per_device(
        tokens, routes, in_gain, group_router, expert_router, w_gate, w_up, w_down, out_gain
    ):
        rows, width = tokens.shape
        top = routes.shape[1]
        hidden = w_gate.shape[2]
        feats = out_gain.shape[0]
        half = chips // 2
        subs = 4
        all_rows = n_ep * rows
        block = 4 * rows
        dma, vmem = pltpu.SemaphoreType.DMA, pltpu.VMEM
        turned = pl.pallas_call(
            functools.partial(layer_kernel, n_ep),
            out_shape=jax.ShapeDtypeStruct((feats, all_rows), BF16),
            in_specs=[pl.BlockSpec(memory_space=pl.ANY)] * 9,
            out_specs=pl.BlockSpec(memory_space=vmem),
            scratch_shapes=[
                vmem((rows, width), BF16),
                vmem((top, rows), jnp.int32),
                vmem((1, width), F32),
                vmem((n_ep + 8, width), F32),
                vmem((1, feats), F32),
                vmem(w_gate.shape, BF16),
                vmem(w_up.shape, BF16),
                vmem(w_down.shape, BF16),
                vmem((chips, rows, width), BF16),
                vmem((chips, rows, width), BF16),
                vmem((chips, 8, LANES), F32),
                vmem((chips, 8, LANES), F32),
                vmem((block, hidden), F32),
                vmem((block, hidden), BF16),
                vmem((chips, rows, width), F32),
                vmem((chips, rows, width), BF16),
                vmem((chips, rows, width), BF16),
                vmem((chips * subs, chips // subs, rows, LANES), BF16),
                vmem((chips * subs, chips // subs, rows, LANES), BF16),
                vmem((2, chips, rows, LANES), F32),
                vmem((feats, all_rows), F32),
                vmem((chips, subs, LANES), F32),
                vmem((2, subs, LANES), F32),
                dma((6,)),
                dma((3,)),
                dma((2, half, subs)),
                dma((2, half)),
                dma((chips,)),
                dma((chips,)),
                dma,
                dma((chips * subs,)),
                dma,
                dma,
                dma,
            ] + [dma] * 9,
            compiler_params=pltpu.CompilerParams(collective_id=0, has_side_effects=True),
        )(
            tokens, routes.T, in_gain.reshape(1, width), group_router.T, expert_router.T,
            w_gate, w_up, w_down, out_gain.reshape(1, feats),
        )
        return turned.T

    in_specs = (
        P(("grp", "ep"), None),
        P(("grp", "ep"), None),
        P(),
        P(),
        P(),
        P("ep", None, None),
        P("ep", None, None),
        P("ep", None, None),
        P("ep"),
    )
    return jax.shard_map(
        per_device, mesh=mesh, in_specs=in_specs, out_specs=P("grp", "ep"), check_vma=False
    )
```

time: 174 us -> 87 us (0.50)
  blocking collectives: 93.8 us -> 0 us
  Pallas kernels: 0 us -> 85.3 us
  waiting for transfers between devices: 50.4 us -> 0 us
  local copies, waits for them, and re-layouts: 12.8 us -> 1.57 us
  matrix products: 6.98 us -> 0 us
  other arithmetic: 4.58 us -> 0 us
  starting transfers between devices: 4.46 us -> 0 us
    all_to_all x2 -> x0, blocking collectives: 93.8 us -> none  [the longest x1 73.9 us: per_device(): lax.all_to_all(outgoing, 'ep', split_axis=0, concat_axis=0, tiled=True)]
    pallas_call x0 -> x1, Pallas kernels: none -> 85.3 us  [per_device(): pl.pallas_call(functools.partial(layer_kernel, n_ep), out_shape=jax.Shape...]
    all_to_all x1 -> x0, waiting for transfers between devices: 50.4 us -> none  [per_device(): lax.all_to_all(answer, 'ep', split_axis=0, concat_axis=0, tiled=True)]
    dot_general x4 -> x0, matrix products: 6.98 us -> none  [the longest x1 4.01 us: expert_rows(): jnp.dot(hidden, w_down[0], preferred_element_type=jnp.float32)]
    gather x12 -> x0, local copies, waits for them, and re-layouts: 6.64 us -> none  [the longest x5 1.88 us: gate_values(): jnp.take_along_axis(group_prob, routes // per_group, axis=1) * expert_prob]
    all_to_all x1 -> x0, starting transfers between devices: 4.46 us -> none  [per_device(): lax.all_to_all(answer, 'ep', split_axis=0, concat_axis=0, tiled=True)]
    convert_element_type x3 -> x0, local copies, waits for them, and re-layouts: 2.26 us -> none  [the longest x1 1.37 us: per_device(): weighted = pair_rows.astype(jnp.float32) * weights.reshape(-1)[:, None]]
    reduce_sum x5 -> x0, other arithmetic: 2.09 us -> none  [the longest x1 1.04 us: normalize(): jnp.mean(values * values, axis=1, keepdims=True) + EPSILON]
  transfers between devices with their start and end apart: 1 -> 0, of which waited for: 1 -> 0; matrix products, arithmetic and copies ran while one was open for 3% -> 0% of each run, Pallas kernels for 0% -> 0%
where the time goes in v1:
time: 87 us; the launch traced here: 86.9 us
  Pallas kernels  85.3 us (98%)
  local copies, waits for them, and re-layouts  1.57 us (2%)
    pallas_call x1, Pallas kernels, per_device(): pl.pallas_call(functools.partial(layer_kernel, n_ep), out_shape=jax.Shape...  85.3 us

profile of v1, /device:TPU:69, one launch (start us, length us, event | category | flops | bytes accessed | tf_op | source)
XLA Modules:
  0.0 86.9 jit_solution(4164898400502906346)
XLA Ops:
  0.0 85.3 %shard_map.91 = bf16[64,1024]{1,0:T(8,128)(2,1)} custom-call(bf16[32,2048]{1,0:T(8,128)(2,1)} %tok_hbm.1, s32[4,32]{1,0:T(4,128)} %bitcast.10, f32[1,2048]{1,0:T(1,128)} %bitcast.9, f32[4,2048]{1,0:T(4,128)} %bitcast.8, f32[32,2048]{1,0:T(8,128)} %bitcast.7, bf16[1,2048,512]{2,1,0:T(8,128)(2,1)} %wg_hbm.1, bf16[1,2048,512]{2,1,0:T(8,128)(2,1)} %wu_hbm.1, ...), custom_call_target="tpu_custom_call" | custom-call | tf_op jit(solution)/shard_map/pallas_call | solution.py:341
  85.3 1.6 %copy.11 = bf16[1024,64]{0,1:T(8,128)(2,1)} copy(bf16[1024,64]{0,1:T(8,128)(2,1)} %bitcast.6) | data formatting | bytes 262144
